TPU v7x, 32 devices: a whole 2x2x4 slice. The times are simulated.
32 devices in a mesh: sp: 16 (over z, y, core), tp: 2 (over x).
Axes of the slice: x: 2, y: 2, z: 4, core: 2. Of those that a mesh axis runs over, the one named last changes fastest.
Arguments:
- queries: bfloat16 [8192, 1024], P('sp', 'tp'), may hold values from -260 to 260, as said below
- keys: bfloat16 [8192, 512], P('sp', 'tp'), may hold values from -8 to 8, as said below
- values: bfloat16 [8192, 512], P('sp', 'tp'), may hold values from -24 to 24
- doc_ids: int32 [8192], P('sp'), may hold values from 0 to 3, never falling along the last dimension, each value on 1 to 4096 neighbouring positions
- sink_logit: float32 [8], P('tp'), may hold values from 2 to 7
- residual_in: bfloat16 [8192, 2048], P(('sp', 'tp')), may hold values from -6 to 6
- w_out: bfloat16 [1024, 2048], replicated, may hold values from -0.375 to 0.375
- gain_one: float32 [2048], replicated, may hold values from 0.1 to 1.9
- w_gate: bfloat16 [2048, 5632], P('sp', 'tp'), may hold values from -0.125 to 0.125
- w_up: bfloat16 [2048, 5632], P('sp', 'tp'), may hold values from -0.125 to 0.125
- w_down: bfloat16 [5632, 2048], P('tp', 'sp'), may hold values from -0.078125 to 0.078125
- gain_two: float32 [2048], replicated, may hold values from 0.1 to 1.9
Outputs:
- layer_out: bfloat16 [8192, 2048], P(('sp', 'tp'))
Inputs may be any that keep to these rules, and one draw needn't show every extreme that they name: Real-valued projected queries. Real-valued projected keys. `doc_ids`: document numbers never fall along the sequence; each document is one run of positions.
All inputs are finite; a program needn't handle non-finite values.
Results may differ from a plain program's by a relative error of at most 0.012.
Values may be sent and summed in bfloat16 or wider, within the bound.
A program may use at most 128 MiB of HBM per device.

v0:
```python
import math

import jax
import jax.numpy as jnp
from jax import lax
from jax.sharding import PartitionSpec as P

HEAD = 128
HALF = 128


ALPHA = 2.0**0.5
EPS = 1e-05
NEGATIVE = -1e30


def shifted(value, axis, steps):
    count = lax.axis_size(axis)
    leading, last = (max(0, -steps), min(count, count - steps))
    return lax.ppermute(value, axis, [(source, source + steps) for source in range(leading, last)])


def layer_norm(values_in, gain):
    average = jnp.mean(values_in, -1, keepdims=True)
    centred = values_in - average
    variance = jnp.mean(centred * centred, -1, keepdims=True)
    return centred * lax.rsqrt(variance + EPS) * gain


def per_device(
    queries,
    keys,
    values,
    doc_ids,
    sink_logit,
    residual_in,
    w_out,
    gain_one,
    w_gate,
    w_up,
    w_down,
    gain_two,
):
    row_count = queries.shape[0]
    sp_size = lax.axis_size("sp")
    kv_local = keys.shape[1] // HEAD
    repeat = queries.shape[1] // keys.shape[1]
    lower = (keys[row_count - HALF :], values[row_count - HALF :], doc_ids[row_count - HALF :])
    upper = (keys[:HALF], values[:HALF], doc_ids[:HALF])
    before = shifted((lower[0], lower[1], lower[2]), "sp", 1)
    after = shifted((upper[0], upper[1], upper[2]), "sp", -1)
    keys_all = jnp.concatenate([before[0], keys, after[0]], 0)
    values_all = jnp.concatenate([before[1], values, after[1]], 0)
    docs_all = jnp.concatenate([before[2], doc_ids, after[2]], 0)
    first_pos = lax.axis_index("sp") * row_count
    block = math.gcd(512, row_count)
    span = block + 2 * HALF
    sinks = sink_logit.reshape(kv_local, repeat)

    def one_block(index):
        start = index * block
        query_blk = queries.reshape(block, kv_local, repeat, HEAD)
        key_blk = keys_all.reshape(span, kv_local, HEAD)
        value_blk = values_all.reshape(span, kv_local, HEAD)
        pos_query = first_pos + start + jnp.arange(block, dtype=jnp.int32)
        pos_key = first_pos + start - HALF + jnp.arange(span, dtype=jnp.int32)
        offset = pos_key[None, :] - pos_query[:, None]
        allowed = (jnp.abs(offset) <= HALF) & (docs_all[None, :] == doc_ids[:, None])
        allowed = allowed & (pos_key[None, :] >= 0) & (pos_key[None, :] < sp_size * row_count)
        scores = jnp.einsum(
            "qgrd,kgd->grqk", query_blk, key_blk, preferred_element_type=jnp.float32
        ) * HEAD ** (-0.5)
        scores = jnp.where(allowed[None, None], scores, NEGATIVE)
        top = jnp.maximum(jnp.max(scores, -1), sinks[:, :, None])
        weights = jnp.exp(scores - top[..., None])
        total = jnp.sum(weights, -1) + jnp.exp(sinks[:, :, None] - top)
        summed = jnp.einsum(
            "grqk,kgd->qgrd",
            weights.astype(jnp.bfloat16),
            value_blk,
            preferred_element_type=jnp.float32,
        )
        scaled = summed / jnp.transpose(total, (2, 0, 1))[..., None]
        return scaled.reshape(block, kv_local * repeat * HEAD).astype(jnp.bfloat16)

    attended = lax.map(one_block, jnp.arange(row_count // block, dtype=jnp.int32)).reshape(
        row_count, -1
    )
    token_rows = lax.all_to_all(attended, "tp", split_axis=0, concat_axis=1, tiled=True)
    mixed_rows = jnp.dot(token_rows, w_out, preferred_element_type=jnp.float32)
    pre_one = ALPHA * residual_in.astype(jnp.float32) + mixed_rows
    normed = layer_norm(pre_one, gain_one).astype(jnp.bfloat16)
    whole_rows = lax.all_gather(normed, "tp", axis=0, tiled=True)
    gate_whole, up_whole = (
        lax.all_gather(w_gate, "sp", axis=0, tiled=True),
        lax.all_gather(w_up, "sp", axis=0, tiled=True),
    )
    gate_part = jnp.dot(whole_rows, gate_whole, preferred_element_type=jnp.float32)
    up_part = jnp.dot(whole_rows, up_whole, preferred_element_type=jnp.float32)
    hidden = (jax.nn.silu(gate_part) * up_part).astype(jnp.bfloat16)
    down_terms = jnp.dot(
        hidden, lax.all_gather(w_down, "sp", axis=1, tiled=True), preferred_element_type=jnp.float32
    )
    rounded = lax.optimization_barrier(down_terms.astype(jnp.bfloat16)).astype(jnp.float32)
    down_rows = lax.psum_scatter(
        rounded.astype(jnp.bfloat16), "tp", scatter_dimension=0, tiled=True
    ).astype(jnp.float32)
    pre_two = ALPHA * normed.astype(jnp.float32) + down_rows
    return layer_norm(pre_two, gain_two).astype(jnp.bfloat16)


def solution(mesh):
    in_specs = (
        P("sp", "tp"),
        P("sp", "tp"),
        P("sp", "tp"),
        P("sp"),
        P("tp"),
        P(("sp", "tp"), None),
        P(),
        P(),
        P("sp", "tp"),
        P("sp", "tp"),
        P("tp", "sp"),
        P(),
    )
    out_specs = P(("sp", "tp"), None)
    return jax.shard_map(
        per_device, mesh=mesh, in_specs=in_specs, out_specs=out_specs, check_vma=False
    )
```

profile of v0, /device:TPU:0, one launch (start us, length us, event | category | flops | bytes accessed | tf_op | source)
XLA Modules:
  0.0 442.6 jit_solution(3270424816436045704)
XLA Ops:
  7.3 2.4 collective-permute-start.2
  9.7 1.3 collective-permute-start.3
  11.0 1.1 copy.17
  12.1 5.2 %collective-permute-start.4 = (bf16[128,256]{0,1:T(8,128)(2,1)S(1)}, bf16[128,256]{0,1:T(8,128)(2,1)S(1)}, u32[]{:S(2)}, u32[]{:S(2)}) collective-permute-start(bf16[128,256]{0,1:T(8,128)(2,1)S(1)} %get-tuple-element.21), channel_id=1, source_target_pairs={{0,2},{2,4},{4,6},{6,8},{8,10},{10,12},{12,14},{14,16},{16,18},{18... | collective-permute-start | bytes 196616 | tf_op jit(solution)/shard_map/ppermute | solution.py:20
  17.3 1.3 collective-permute-start.5
  19.5 4.3 collective-permute-start
  23.8 1.2 reshape.158
  25.1 1.3 collective-permute-start.1
  27.4 1.4 fusion.2
  29.0 1.4 fusion
  30.3 1.2 copy-done.1
  31.8 4.7 %divide_convert_fusion = bf16[512,2,2,128]{0,3,2,1:T(8,128)(2,1)S(1)} fusion(bf16[768,2,128,1]{0,2,3,1:T(8,128)(2,1)S(1)} %bitcast.47, f32[2,768,512,2]{2,1,3,0:T(8,128)} %copy-done.1, f32[2,2,512]{2,1,0:T(2,128)S(1)} %broadcast_maximum_fusion, pred[512,768]{0,1:T(8,128)(4,1)S(1)} %fusion.9, f32[512,2,2]{0,2,1:T(2,128)S(1)} %add_bitcast_fusion), kind=kOutput, calls=%fused_computation.21 | convolution fusion | flops 409468928 | bytes 7618560 | tf_op jit(solution)/shard_map/while/body/eval_jaxpr/grqk,kgd->qgrd/dot_general | solution.py:77
  36.8 10.8 %all_to_all.16 = bf16[2,256,512]{1,2,0:T(8,128)(2,1)S(1)} all-to-all(bf16[2,256,512]{1,2,0:T(8,128)(2,1)S(1)} %copy.23), channel_id=1, replica_groups=mesh['sp'=16,'tp'=2] {'tp'}, dimensions={0} | all-to-all | bytes 1048576 | tf_op jit(solution)/shard_map/all_to_all | solution.py:89
  47.6 3.6 fusion.25
  51.9 1.3 multiply_convert_fusion.2
  55.3 34.1 %all-gather.5.cloned.1.call-done = bf16[512,2048]{1,0:T(8,128)(2,1)} async-done(((bf16[256,2048]{1,0:T(8,128)(2,1)}), bf16[512,2048]{1,0:T(8,128)(2,1)}) %all-gather.5.cloned.1.call-update) | async-done | bytes 2097168 | tf_op jit(solution)/shard_map/all_gather | solution.py:93
  89.4 96.3 %all-gather.7.cloned.1.call-done = bf16[2048,2816]{1,0:T(8,128)(2,1)} async-done(((bf16[128,2816]{1,0:T(8,128)(2,1)}), bf16[2048,2816]{1,0:T(8,128)(2,1)}) %all-gather.7.cloned.1.call-update) | async-done | bytes 11534352 | tf_op jit(solution)/shard_map/all_gather | solution.py:95
  185.7 12.5 %fusion.26 = f32[512,2816]{1,0:T(8,128)} fusion(bf16[512,2048]{1,0:T(8,128)(2,1)} %all-gather.5.cloned.1.call-done, bf16[2048,2816]{1,0:T(8,128)(2,1)} %all-gather.7.cloned.1.call-done), kind=kOutput, calls=%fused_computation.44 | convolution fusion | flops 5905580032 | bytes 19398656 | tf_op jit(solution)/shard_map/dot_general | solution.py:98
  198.2 84.9 %all-gather.11.cloned.1.call-done = bf16[2816,2048]{1,0:T(8,128)(2,1)} async-done(((bf16[2816,128]{1,0:T(8,128)(2,1)}), bf16[2816,2048]{1,0:T(8,128)(2,1)}) %all-gather.11.cloned.1.call-update) | async-done | bytes 11534352 | tf_op jit(solution)/shard_map/all_gather | solution.py:102
  283.1 94.3 %all-gather.9.cloned.1.call-done = bf16[2048,2816]{1,0:T(8,128)(2,1)} async-done(((bf16[128,2816]{1,0:T(8,128)(2,1)}), bf16[2048,2816]{1,0:T(8,128)(2,1)}) %all-gather.9.cloned.1.call-update) | async-done | bytes 11534352 | tf_op jit(solution)/shard_map/all_gather | solution.py:96
  377.4 23.3 %convolution_convert_fusion = bf16[512,2048]{1,0:T(8,128)(2,1)} fusion(bf16[2816,2048]{1,0:T(8,128)(2,1)} %all-gather.11.cloned.1.call-done, f32[512,2816]{1,0:T(8,128)} %fusion.26, bf16[512,2048]{1,0:T(8,128)(2,1)} %all-gather.5.cloned.1.call-done, bf16[2048,2816]{1,0:T(8,128)(2,1)} %all-gather.9.cloned.1.call-done), kind=kOutput, calls=%fused_computation.8 | convolution fusion | flops 11820859392 | bytes 33030144 | tf_op jit(solution)/shard_map/dot_general | solution.py:101
  400.7 30.3 %reduce-scatter.2.cloned.1.call-done = bf16[256,2048]{1,0:T(8,128)(2,1)} async-done(((bf16[512,2048]{1,0:T(8,128)(2,1)}), bf16[256,2048]{1,0:T(8,128)(2,1)}) %reduce-scatter.2.cloned.1.call-update) | async-done | bytes 1048592 | tf_op jit(solution)/shard_map/reduce_scatter | solution.py:105
  431.0 1.9 fusion.6
  433.8 2.3 multiply_convert_fusion.1
  (53 shorter events, 6.9 us)
Async XLA Ops:
  6.5 19.9 %copy-start.5 = (s32[512]{0:T(512)S(1)}, s32[512]{0:T(512)}, u32[]{:S(2)}) copy-start(s32[512]{0:T(512)} %param.15) | copy-start | bytes 6148
  6.5 18.5 %copy-start.7 = (f32[4]{0:T(128)S(1)}, f32[4]{0:T(128)}, u32[]{:S(2)}) copy-start(f32[4]{0:T(128)} %param.16) | copy-start | bytes 52
  6.5 82.9 %all-gather.5.cloned.1.call-start = ((), (), s32[]{:S(2)}) async-start(), calls=%async_computation.2 | async-start | bytes 3145728 | tf_op jit(solution)/shard_map/all_gather | solution.py:93
  7.3 17.8 %collective-permute-start.2 = (s32[128]{0:T(128)S(1)}, s32[128]{0:T(128)S(1)}, u32[]{:S(2)}, u32[]{:S(2)}) collective-permute-start(s32[128]{0:T(128)S(1)} %get-tuple-element.25), channel_id=1, source_target_pairs={{0,2},{2,4},{4,6},{6,8},{8,10},{10,12},{12,14},{14,16},{16,18},{18... | collective-permute-start | bytes 1544 | tf_op jit(solution)/shard_map/ppermute | solution.py:20
  9.7 16.7 %collective-permute-start.3 = (s32[128]{0:T(128)S(1)}, s32[128]{0:T(128)S(1)}, u32[]{:S(2)}, u32[]{:S(2)}) collective-permute-start(s32[128]{0:T(128)S(1)} %get-tuple-element.26), channel_id=1, source_target_pairs={{2,0},{4,2},{6,4},{8,6},{10,8},{12,10},{14,12},{16,14},{18,16},{20... | collective-permute-start | bytes 1544 | tf_op jit(solution)/shard_map/ppermute | solution.py:20
  12.1 15.2 %collective-permute-start.4 = (bf16[128,256]{0,1:T(8,128)(2,1)S(1)}, bf16[128,256]{0,1:T(8,128)(2,1)S(1)}, u32[]{:S(2)}, u32[]{:S(2)}) collective-permute-start(bf16[128,256]{0,1:T(8,128)(2,1)S(1)} %get-tuple-element.21), channel_id=1, source_target_pairs={{0,2},{2,4},{4,6},{6,8},{8,10},{10,12},{12,14},{14,16},{16,18},{18... | collective-permute-start | bytes 196616 | tf_op jit(solution)/shard_map/ppermute | solution.py:20
  17.3 10.1 %collective-permute-start.5 = (bf16[128,256]{0,1:T(8,128)(2,1)S(1)}, bf16[128,256]{0,1:T(8,128)(2,1)S(1)}, u32[]{:S(2)}, u32[]{:S(2)}) collective-permute-start(bf16[128,256]{0,1:T(8,128)(2,1)S(1)} %get-tuple-element.22), channel_id=1, source_target_pairs={{2,0},{4,2},{6,4},{8,6},{10,8},{12,10},{14,12},{16,14},{18,16},{20... | collective-permute-start | bytes 196616 | tf_op jit(solution)/shard_map/ppermute | solution.py:20
  19.5 12.1 %collective-permute-start = (bf16[128,256]{1,0:T(8,128)(2,1)S(1)}, bf16[128,256]{1,0:T(8,128)(2,1)S(1)}, u32[]{:S(2)}, u32[]{:S(2)}) collective-permute-start(bf16[128,256]{1,0:T(8,128)(2,1)S(1)} %get-tuple-element.23), channel_id=1, source_target_pairs={{0,2},{2,4},{4,6},{6,8},{8,10},{10,12},{12,14},{14,16},{16,18},{18... | collective-permute-start | bytes 196616 | tf_op jit(solution)/shard_map/ppermute | solution.py:20
  25.1 6.5 %collective-permute-start.1 = (bf16[128,256]{1,0:T(8,128)(2,1)S(1)}, bf16[128,256]{1,0:T(8,128)(2,1)S(1)}, u32[]{:S(2)}, u32[]{:S(2)}) collective-permute-start(bf16[128,256]{1,0:T(8,128)(2,1)S(1)} %get-tuple-element.24), channel_id=1, source_target_pairs={{2,0},{4,2},{6,4},{8,6},{10,8},{12,10},{14,12},{16,14},{18,16},{20... | collective-permute-start | bytes 196616 | tf_op jit(solution)/shard_map/ppermute | solution.py:20
  28.9 2.6 copy-start.1
  29.0 2.7 copy-start.3
  36.5 11.1 %copy-start.2 = (bf16[256,2048]{1,0:T(8,128)(2,1)S(1)}, bf16[256,2048]{1,0:T(8,128)(2,1)}, u32[]{:S(2)}) copy-start(bf16[256,2048]{1,0:T(8,128)(2,1)} %param.17) | copy-start | bytes 3145732
  51.1 0.7 copy-start.4
  53.2 132.5 %all-gather.7.cloned.1.call-start = ((), (), s32[]{:S(2)}) async-start(), calls=%async_computation.3 | async-start | bytes 12255232 | tf_op jit(solution)/shard_map/all_gather | solution.py:95
  54.0 229.1 %all-gather.11.cloned.1.call-start = ((), (), s32[]{:S(2)}) async-start(), calls=%async_computation.5 | async-start | bytes 12255232 | tf_op jit(solution)/shard_map/all_gather | solution.py:102
  54.7 322.7 %all-gather.9.cloned.1.call-start = ((), (), s32[]{:S(2)}) async-start(), calls=%async_computation.4 | async-start | bytes 12255232 | tf_op jit(solution)/shard_map/all_gather | solution.py:96
  55.3 375.8 %reduce-scatter.2.cloned.1.call-start = ((), (), s32[]{:S(2)}) async-start(), calls=%async_computation.6 | async-start | bytes 3145728 | tf_op jit(solution)/shard_map/reduce_scatter | solution.py:105
  431.0 2.0 copy-start
  433.0 0.8 copy-start.6
Sparse Core Ops, SparseCore 0:
  53.3 36.0 all-gather.4
  91.7 93.9 all-gather.6
  187.9 95.1 all-gather.10
  285.2 92.1 all-gather.8
  400.8 30.1 reduce-scatter.1
where the time goes:
time: 443 us
  waiting for transfers between devices  342 us (77%)
  matrix products  45.5 us (10%)
  starting transfers between devices  15.8 us (4%)
  between operations  13.4 us (3%)
  blocking collectives  10.8 us (2%)
  other arithmetic  9.3 us (2%)
  local copies, waits for them, and re-layouts  5.92 us (1%)
    all_gather x1, waiting for transfers between devices, per_device(): lax.all_gather(w_gate, 'sp', axis=0, tiled=True)  96.3 us
    all_gather x1, waiting for transfers between devices, per_device(): lax.all_gather(w_up, 'sp', axis=0, tiled=True)  94.3 us
    all_gather x1, waiting for transfers between devices, per_device(): lax.all_gather(w_down, 'sp', axis=1, tiled=True)  84.9 us
    all_gather x1, waiting for transfers between devices, per_device(): whole_rows = lax.all_gather(normed, 'tp', axis=0, tiled=True)  34.1 us
    reduce_scatter x1, waiting for transfers between devices, per_device(): lax.psum_scatter(rounded.astype(jnp.bfloat16), 'tp', scatter_dimension=0,...  30.3 us
    dot_general x1, matrix products, per_device(): jnp.dot(hidden, lax.all_gather(w_down, 'sp', axis=1, tiled=True), preferr...  23.3 us
    ppermute x6, starting transfers between devices, shifted(): lax.ppermute(value, axis, [(source, source + steps) for source in range(l...  15.7 us
    dot_general x1, matrix products, per_device(): jnp.dot(whole_rows, gate_whole, preferred_element_type=jnp.float32)  12.5 us
  transfers between devices with their start and end apart: 11, of which 5 were waited for; matrix products, arithmetic and copies ran while one was open for 4% of the time, Pallas kernels for 0%

commit v1 on v0

v1 whole, which is shorter than its diff:
```python
import functools
import math

import jax
import jax.numpy as jnp
from jax import lax
from jax.experimental import pallas as pl
from jax.experimental.pallas import tpu as pltpu
from jax.sharding import PartitionSpec as P

HEAD = 128
HALF = 128
CORES = 2
ALPHA = 2.0**0.5
EPS = 1e-05
NEGATIVE = -1e30
MESH = pl.DeviceIdType.MESH


def layer_norm(values_in, gain):
    average = jnp.mean(values_in, -1, keepdims=True)
    centred = values_in - average
    variance = jnp.mean(centred * centred, -1, keepdims=True)
    return centred * lax.rsqrt(variance + EPS) * gain


def kernel(
    sp_size,
    tp_size,
    q_ref,
    doc_col_ref,
    sink_ref,
    res_ref,
    gain_one_ref,
    gain_two_ref,
    k_hbm,
    v_hbm,
    doc_row_hbm,
    w_out_hbm,
    wg_hbm,
    wu_hbm,
    wd_hbm,
    out_ref,
    k_all,
    v_all,
    doc_all,
    w_out,
    gate_w,
    up_w,
    down_w,
    att,
    tokens,
    pre,
    normed,
    hidden,
    parts,
    others,
    local_sem,
    halo_send,
    halo_recv,
    ring_send,
    ring_recv,
    pair_send,
    pair_recv,
    tok_send,
    tok_recv,
    norm_send,
    norm_recv,
    sum_send,
    sum_recv,
):
    sp = lax.axis_index("sp")
    tp = lax.axis_index("tp")
    chips = sp_size // CORES
    y_size = math.gcd(tp_size, chips)
    z_size = chips // y_size
    half_ring = chips // 2
    core = lax.rem(sp, CORES)
    chip = sp // CORES
    my_y = lax.rem(chip, y_size)
    my_z = chip // y_size
    odd = lax.rem(my_y, 2)
    pos = my_y * z_size + my_z * (1 - odd) + (z_size - 1 - my_z) * odd

    def chip_at(steps):
        p = lax.rem(pos + (chips + steps), chips)
        y = p // z_size
        along = lax.rem(p, z_size)
        turned = lax.rem(y, 2)
        z = along * (1 - turned) + (z_size - 1 - along) * turned
        return z * y_size + y

    rows = q_ref.shape[0]
    token_rows = res_ref.shape[0]
    depth = wg_hbm.shape[0]
    cols_tp = q_ref.shape[1]
    kv_local = k_hbm.shape[1] // HEAD
    repeat = q_ref.shape[1] // k_hbm.shape[1]
    width = res_ref.shape[1]

    forward = (chip_at(1) * CORES + core, tp)
    backward = (chip_at(-1) * CORES + core, tp)
    partner = (chip * CORES + (1 - core), tp)
    after = (lax.rem(sp + 1, sp_size), tp)
    before = (lax.rem(sp + sp_size - 1, sp_size), tp)
    peers = [lax.rem(tp + i, tp_size) for i in range(1, tp_size)]

    barrier = pltpu.get_barrier_semaphore()
    greeted = [forward, backward, partner, after, before] + [(sp, j) for j in peers]
    for device in greeted:
        pl.semaphore_signal(barrier, inc=1, device_id=device, device_id_type=MESH)

    loads = [
        pltpu.make_async_copy(k_hbm, k_all.at[pl.ds(HALF, rows)], local_sem.at[0]),
        pltpu.make_async_copy(v_hbm, v_all.at[pl.ds(HALF, rows)], local_sem.at[1]),
        pltpu.make_async_copy(doc_row_hbm, doc_all.at[:, pl.ds(HALF, rows)], local_sem.at[2]),
        pltpu.make_async_copy(w_out_hbm, w_out, local_sem.at[3]),
    ]
    mine = pl.multiple_of(sp * depth, depth)
    own_loads = [
        pltpu.make_async_copy(src, dst.at[pl.ds(mine, depth)], local_sem.at[4 + i])
        for i, (src, dst) in enumerate(((wg_hbm, gate_w), (wu_hbm, up_w), (wd_hbm, down_w)))
    ]
    for load in loads + own_loads:
        load.start()
    pl.semaphore_wait(barrier, len(greeted))

    def remote(src, dst, send, recv, device):
        return pltpu.make_async_remote_copy(
            src_ref=src, dst_ref=dst, send_sem=send, recv_sem=recv, device_id=device, device_id_type=MESH
        )

    low, high = (pl.ds(0, HALF), pl.ds(rows - HALF, HALF))
    into_low, into_high = (pl.ds(0, HALF), pl.ds(HALF + rows, HALF))
    halos = []
    for i, (src, dst) in enumerate(((k_hbm, k_all), (v_hbm, v_all))):
        halos.append(
            remote(src.at[high], dst.at[into_low], halo_send.at[i, 0], halo_recv.at[i, 0], after)
        )
        halos.append(
            remote(src.at[low], dst.at[into_high], halo_send.at[i, 1], halo_recv.at[i, 1], before)
        )
    halos.append(
        remote(
            doc_row_hbm.at[:, high], doc_all.at[:, into_low], halo_send.at[2, 0], halo_recv.at[2, 0], after
        )
    )
    halos.append(
        remote(
            doc_row_hbm.at[:, low], doc_all.at[:, into_high], halo_send.at[2, 1], halo_recv.at[2, 1], before
        )
    )
    for halo in halos:
        halo.start()

    part_rows = depth // 2
    pieces = (
        (wg_hbm, gate_w, 0, depth),
        (wu_hbm, up_w, 0, depth),
        (wd_hbm, down_w, 0, part_rows),
        (wd_hbm, down_w, part_rows, part_rows),
    )

    def place(piece, chip_id, core_id):
        _, buf, first, count = pieces[piece]
        start = pl.multiple_of((chip_id * CORES + core_id) * depth + first, count)
        return buf.at[pl.ds(start, count)]

    def own(piece):
        src, _, first, count = pieces[piece]
        return src.at[pl.ds(first, count)]

    def ring_out(way, piece, distance):
        steps = -(distance - 1) if way == 0 else distance - 1
        dst = place(piece, chip_at(steps), core)
        src = own(piece) if distance == 1 else dst
        return remote(
            src,
            dst,
            ring_send.at[way, piece, distance],
            ring_recv.at[way, piece, distance],
            forward if way == 0 else backward,
        )

    def ring_in(way, piece, distance):
        dst = place(piece, chip_at(-distance if way == 0 else distance), core)
        return remote(
            dst,
            dst,
            ring_send.at[way, piece, distance],
            ring_recv.at[way, piece, distance],
            backward if way == 0 else forward,
        )

    def pair(way, piece, distance, core_id):
        steps = 0 if distance == 0 else (-distance if way == 0 else distance)
        dst = place(piece, chip_at(steps), core_id)
        src = own(piece) if distance == 0 else dst
        return remote(
            src, dst, pair_send.at[way, piece, distance], pair_recv.at[way, piece, distance], partner
        )

    def pair_in(way, piece, distance):
        steps = 0 if distance == 0 else (-distance if way == 0 else distance)
        dst = place(piece, chip_at(steps), 1 - core)
        return remote(
            dst, dst, pair_send.at[way, piece, distance], pair_recv.at[way, piece, distance], partner
        )

    sent = []

    def launch(copy):
        copy.start()
        sent.append(copy)

    rounds = []
    for both in ((0, 1), (2, 3)):
        for distance in range(1, half_ring + 1):
            rounds.append((distance, both[0], both[1]))
            if distance < half_ring:
                rounds.append((distance, both[1], both[0]))
    legs = [set(), set()]
    for distance, first, second in rounds:
        legs[0].add((distance, first))
        legs[1].add((distance, second))
    per_phase = len(rounds) // 2

    def pump(index):
        distance, first, second = rounds[index]
        for way, piece in ((0, first), (1, second)):
            ring_in(way, piece, distance).wait_recv()
            if (distance + 1, piece) in legs[way]:
                launch(ring_out(way, piece, distance + 1))
            launch(pair(way, piece, distance, core))
        if index == per_phase - 2:
            launch(ring_out(0, 2, 1))
            launch(ring_out(1, 3, 1))
        if index == per_phase - 1:
            launch(ring_out(0, 3, 1))
            launch(ring_out(1, 2, 1))

    launch(ring_out(0, 0, 1))
    launch(ring_out(1, 1, 1))
    launch(ring_out(0, 1, 1))
    launch(ring_out(1, 0, 1))
    for piece in range(4):
        launch(pair(0, piece, 0, core))

    for load in loads[:3]:
        load.wait()
    for halo in halos:
        halo.wait_recv()
    span = rows + 2 * HALF
    at = lax.broadcasted_iota(jnp.int32, (1, span), 1) + (sp * rows - HALF)
    inside = jnp.logical_and(at >= 0, at < sp_size * rows)
    doc_keys = jnp.where(inside, doc_all[...], -1)
    reach = 3 * HALF
    offset = lax.broadcasted_iota(jnp.int32, (HALF, reach), 1) - lax.broadcasted_iota(
        jnp.int32, (HALF, reach), 0
    )
    near = jnp.logical_and(offset >= 0, offset <= 2 * HALF)
    for block in range(rows // HALF):
        doc_query = doc_col_ref[block * HALF : (block + 1) * HALF, :]
        same = doc_query == doc_keys[:, block * HALF : block * HALF + reach]
        allowed = jnp.logical_and(near, same)
        for group in range(kv_local):
            lanes = slice(group * HEAD, (group + 1) * HEAD)
            key_blk = k_all[block * HALF : block * HALF + reach, lanes]
            value_blk = v_all[block * HALF : block * HALF + reach, lanes]
            for r in range(repeat):
                h = group * repeat + r
                query_blk = q_ref[block * HALF : (block + 1) * HALF, h * HEAD : (h + 1) * HEAD]
                scores = lax.dot_general(
                    query_blk, key_blk, (((1,), (1,)), ((), ())), preferred_element_type=jnp.float32
                ) * HEAD ** (-0.5)
                scores = jnp.where(allowed, scores, NEGATIVE)
                sink = sink_ref[h : h + 1, 0:1]
                top = jnp.maximum(jnp.max(scores, -1, keepdims=True), sink)
                weights = jnp.exp(scores - top)
                total = jnp.sum(weights, -1, keepdims=True) + jnp.exp(sink - top)
                summed = jnp.dot(
                    weights.astype(jnp.bfloat16), value_blk, preferred_element_type=jnp.float32
                )
                att[block * HALF : (block + 1) * HALF, h * HEAD : (h + 1) * HEAD] = (
                    summed / total
                ).astype(jnp.bfloat16)

    my_rows = pl.ds(pl.multiple_of(tp * token_rows, token_rows), token_rows)
    tokens[pl.ds(tp, 1)] = att[my_rows, :][None]
    pump(0)
    for i, j in enumerate(peers):
        launch(
            remote(
                att.at[pl.ds(pl.multiple_of(j * token_rows, token_rows), token_rows)],
                tokens.at[tp],
                tok_send.at[i],
                tok_recv.at[i],
                (sp, j),
            )
        )
    loads[3].wait()
    for i in range(tp_size - 1):
        source = lax.rem(tp + (tp_size - 1 - i), tp_size)
        slot = tokens.at[source]
        remote(slot, slot, tok_send.at[i], tok_recv.at[i], (sp, source)).wait_recv()
    tile = min(512, width)

    @pl.loop(0, width // tile)
    def _(t):
        lanes = pl.ds(pl.multiple_of(t * tile, tile), tile)
        mixed = ALPHA * res_ref[:, lanes].astype(jnp.float32)
        for j in range(tp_size):
            mixed += jnp.dot(
                tokens[j],
                w_out[j * cols_tp : (j + 1) * cols_tp, lanes],
                preferred_element_type=jnp.float32,
            )
        pre[:, lanes] = mixed

    strip = math.gcd(32, token_rows)

    @pl.loop(0, token_rows // strip)
    def _(t):
        here = pl.ds(pl.multiple_of(t * strip, strip), strip)
        there = pl.ds(pl.multiple_of(tp * token_rows + t * strip, strip), strip)
        normed[there, :] = layer_norm(pre[here, :], gain_one_ref[...]).astype(jnp.bfloat16)

    pump(1)
    for i, j in enumerate(peers):
        launch(
            remote(
                normed.at[my_rows], normed.at[my_rows], norm_send.at[i], norm_recv.at[i], (sp, j)
            )
        )
    for index in range(2, per_phase):
        pump(index)

    for load in own_loads:
        load.wait()
    for piece in (0, 1):
        pair_in(0, piece, 0).wait_recv()
    for distance, first, second in rounds[:per_phase]:
        pair_in(0, first, distance).wait_recv()
        pair_in(1, second, distance).wait_recv()
    for i in range(tp_size - 1):
        source = lax.rem(tp + (tp_size - 1 - i), tp_size)
        slot = normed.at[pl.ds(pl.multiple_of(source * token_rows, token_rows), token_rows)]
        remote(slot, slot, norm_send.at[i], norm_recv.at[i], (sp, source)).wait_recv()

    units = wg_hbm.shape[1]
    block_units = 256 if units % 256 == 0 else 128
    steps = units // block_units

    def hidden_tiles(first, last):
        @pl.loop(first, last)
        def _(t):
            lanes = pl.ds(pl.multiple_of(t * block_units, block_units), block_units)
            gate = jnp.dot(normed[...], gate_w[:, lanes], preferred_element_type=jnp.float32)
            up = jnp.dot(normed[...], up_w[:, lanes], preferred_element_type=jnp.float32)
            hidden[:, lanes] = (gate / (1.0 + jnp.exp(-gate)) * up).astype(jnp.bfloat16)

    middle = steps // 2
    hidden_tiles(0, middle)
    pump(per_phase)
    hidden_tiles(middle, steps)
    pump(per_phase + 1)

    chunk = CORES * depth
    order = []

    def chunk_sends(number, owner):
        lanes = pl.ds(pl.multiple_of(owner * chunk, chunk), chunk)
        for i, j in enumerate(peers):
            launch(
                remote(
                    parts.at[j, :, lanes],
                    others.at[i, :, lanes],
                    sum_send.at[number, i],
                    sum_recv.at[number, i],
                    (sp, j),
                )
            )

    def down_chunk(owner):
        start = pl.multiple_of(owner * chunk, chunk)
        part = lax.dot_general(
            hidden[...],
            down_w[pl.ds(start, chunk), :],
            (((1,), (1,)), ((), ())),
            preferred_element_type=jnp.float32,
        ).astype(jnp.bfloat16)
        for j in range(tp_size):
            parts[j, :, pl.ds(start, chunk)] = part[j * token_rows : (j + 1) * token_rows, :]
        order.append(owner)
        if len(order) > 1:
            chunk_sends(len(order) - 2, order[-2])

    for piece in (2, 3):
        pair_in(0, piece, 0).wait_recv()
    down_chunk(chip_at(0))
    index = per_phase + 2
    for distance in range(1, half_ring + 1):
        if distance == half_ring:
            pump(index)
            index += 1
            pair_in(0, 2, distance).wait_recv()
            pair_in(1, 3, distance).wait_recv()
            down_chunk(chip_at(distance))
            continue
        if distance > 1:
            pump(index)
            pump(index + 1)
            index += 2
        for piece in (2, 3):
            pair_in(0, piece, distance).wait_recv()
            pair_in(1, piece, distance).wait_recv()
        down_chunk(chip_at(-distance))
        down_chunk(chip_at(distance))
    chunk_sends(len(order) - 1, order[-1])
    for number, owner in enumerate(order):
        lanes = pl.ds(pl.multiple_of(owner * chunk, chunk), chunk)
        for i in range(tp_size - 1):
            source = lax.rem(tp + (tp_size - 1 - i), tp_size)
            slot = others.at[i, :, lanes]
            remote(slot, slot, sum_send.at[number, i], sum_recv.at[number, i], (sp, source)).wait_recv()

    @pl.loop(0, token_rows // strip)
    def _(t):
        here = pl.ds(pl.multiple_of(t * strip, strip), strip)
        there = pl.ds(pl.multiple_of(tp * token_rows + t * strip, strip), strip)
        down = parts[pl.ds(tp, 1), here, :][0].astype(jnp.float32)
        for i in range(tp_size - 1):
            down += others[i, here, :].astype(jnp.float32)
        pre_two = ALPHA * normed[there, :].astype(jnp.float32) + down
        out_ref[here, :] = layer_norm(pre_two, gain_two_ref[...]).astype(jnp.bfloat16)

    for halo in halos:
        halo.wait_send()
    for copy in sent:
        copy.wait_send()


def solution(mesh):
    sp_size = mesh.shape["sp"]
    tp_size = mesh.shape["tp"]

    def per_device(
        queries,
        keys,
        values,
        doc_ids,
        sink_logit,
        residual_in,
        w_out,
        gain_one,
        w_gate,
        w_up,
        w_down,
        gain_two,
    ):
        rows = queries.shape[0]
        token_rows, width = residual_in.shape
        units = w_gate.shape[1]
        span = rows + 2 * HALF
        chips = sp_size // CORES
        full = w_gate.shape[0] * sp_size
        bf16, f32 = (jnp.bfloat16, jnp.float32)
        dma = pltpu.SemaphoreType.DMA
        others = max(tp_size - 1, 1)
        vmem, anywhere = (pl.BlockSpec(memory_space=pltpu.VMEM), pl.BlockSpec(memory_space=pl.ANY))
        return pl.pallas_call(
            functools.partial(kernel, sp_size, tp_size),
            out_shape=jax.ShapeDtypeStruct((token_rows, width), bf16),
            in_specs=[vmem] * 6 + [anywhere] * 7,
            out_specs=vmem,
            scratch_shapes=[
                pltpu.VMEM((span, keys.shape[1]), bf16),
                pltpu.VMEM((span, keys.shape[1]), bf16),
                pltpu.VMEM((1, span), jnp.int32),
                pltpu.VMEM(w_out.shape, bf16),
                pltpu.VMEM((full, units), bf16),
                pltpu.VMEM((full, units), bf16),
                pltpu.VMEM((w_down.shape[1] * sp_size, units), bf16),
                pltpu.VMEM((rows, queries.shape[1]), bf16),
                pltpu.VMEM((tp_size, token_rows, queries.shape[1]), bf16),
                pltpu.VMEM((token_rows, width), f32),
                pltpu.VMEM((rows, width), bf16),
                pltpu.VMEM((rows, units), bf16),
                pltpu.VMEM((tp_size, token_rows, width), bf16),
                pltpu.VMEM((others, token_rows, width), bf16),
                dma((7,)),
                dma((3, 2)),
                dma((3, 2)),
                dma((2, 4, chips // 2 + 1)),
                dma((2, 4, chips // 2 + 1)),
                dma((2, 4, chips // 2 + 1)),
                dma((2, 4, chips // 2 + 1)),
                dma((others,)),
                dma((others,)),
                dma((others,)),
                dma((others,)),
                dma((chips, others)),
                dma((chips, others)),
            ],
            compiler_params=pltpu.CompilerParams(
                collective_id=0, has_side_effects=True, vmem_limit_bytes=62 * 2**20
            ),
        )(
            queries,
            doc_ids[:, None],
            jnp.broadcast_to(sink_logit[:, None], (sink_logit.shape[0], HEAD)),
            residual_in,
            gain_one[None, :],
            gain_two[None, :],
            keys,
            values,
            doc_ids[None, :],
            w_out,
            w_gate,
            w_up,
            w_down.T,
        )

    in_specs = (
        P("sp", "tp"),
        P("sp", "tp"),
        P("sp", "tp"),
        P("sp"),
        P("tp"),
        P(("sp", "tp"), None),
        P(),
        P(),
        P("sp", "tp"),
        P("sp", "tp"),
        P("tp", "sp"),
        P(),
    )
    return jax.shard_map(
        per_device, mesh=mesh, in_specs=in_specs, out_specs=P(("sp", "tp"), None), check_vma=False
    )
```

time: 443 us -> 197 us (0.44)
  waiting for transfers between devices: 342 us -> 0 us
  Pallas kernels: 0 us -> 189 us
  matrix products: 45.5 us -> 0 us
  starting transfers between devices: 15.8 us -> 0 us
  between operations: 13.4 us -> 0.01 us
  blocking collectives: 10.8 us -> 0 us
  other arithmetic: 9.3 us -> 0 us
    all_gather x4 -> x0, waiting for transfers between devices: 310 us -> none  [the longest x1 96.3 us: per_device(): lax.all_gather(w_gate, 'sp', axis=0, tiled=True)]
    pallas_call x0 -> x1, Pallas kernels: none -> 189 us  [per_device(): pl.pallas_call(functools.partial(kernel, sp_size, tp_size), out_shape=jax...]
    dot_general x5 -> x0, matrix products: 45.5 us -> none  [the longest x1 23.3 us: per_device(): jnp.dot(hidden, lax.all_gather(w_down, 'sp', axis=1, tiled=True), preferr...]
    reduce_scatter x1 -> x0, waiting for transfers between devices: 30.3 us -> none  [per_device(): lax.psum_scatter(rounded.astype(jnp.bfloat16), 'tp', scatter_dimension=0,...]
    ppermute x6 -> x0, starting transfers between devices: 15.7 us -> none  [shifted(): lax.ppermute(value, axis, [(source, source + steps) for source in range(l...]
    all_to_all x1 -> x0, blocking collectives: 10.8 us -> none  [per_device(): lax.all_to_all(attended, 'tp', split_axis=0, concat_axis=1, tiled=True)]
    reduce_sum x4 -> x0, other arithmetic: 4.43 us -> none  [the longest x1 1.93 us: layer_norm(): average = jnp.mean(values_in, -1, keepdims=True)]
  transfers between devices with their start and end apart: 11 -> 0, of which waited for: 5 -> 0; matrix products, arithmetic and copies ran while one was open for 4% -> 0% of each run, Pallas kernels for 0% -> 0%
where the time goes in v1:
time: 197 us; the launch traced here: 196 us
  Pallas kernels  189 us (96%)
  local copies, waits for them, and re-layouts  7.39 us (4%)
    pallas_call x1, Pallas kernels, per_device(): pl.pallas_call(functools.partial(kernel, sp_size, tp_size), out_shape=jax...  189 us
    unnamed x2, local copies, waits for them, and re-layouts  4.54 us

profile of v1, /device:TPU:0, one launch (start us, length us, event | category | flops | bytes accessed | tf_op | source)
XLA Modules:
  0.0 196.4 jit_solution(15950342536962527614)
XLA Ops:
  0.0 1.3 broadcast_in_dim.19.sink_ref
  1.3 1.6 copy.15.doc_col_ref
  2.8 2.2 %copy.14 = bf16[2816,128]{0,1:T(8,128)(2,1)} copy(bf16[2816,128]{1,0:T(8,128)(2,1)} %param.22) | data formatting | bytes 1441792 | tf_op args[10]
  5.1 189.0 %shard_map.118 = bf16[256,2048]{1,0:T(8,128)(2,1)} custom-call(bf16[512,512]{1,0:T(8,128)(2,1)} %q_ref.1, s32[512,1]{1,0:T(8,128)} %copy.15.doc_col_ref, f32[4,128]{1,0:T(4,128)} %broadcast_in_dim.19.sink_ref, bf16[256,2048]{1,0:T(8,128)(2,1)} %res_ref.1, f32[1,2048]{1,0:T(1,128)} %bitcast.8, f32[1,2048]{1,0:T(1,128)} %bitcast.9, bf16[512,256]{1,0:T(8,128)(2,1)} %k_hbm.1, ...), custom_call_target="tpu_custom_call" | custom-call | tf_op jit(solution)/shard_map/pallas_call | solution.py:471
  194.1 2.3 %copy.17 = bf16[256,2048]{1,0:T(8,128)(2,1)} copy(bf16[256,2048]{1,0:T(8,128)(2,1)} %shard_map.118) | data formatting | bytes 2097152

commit v2 on v1

--- a/solution.py
+++ b/solution.py
@@ -28,7 +28,6 @@
     sp_size,
     tp_size,
     q_ref,
-    doc_col_ref,
     sink_ref,
     res_ref,
     gain_one_ref,
@@ -53,6 +52,7 @@
     pre,
     normed,
     hidden,
+    down_in,
     parts,
     others,
     local_sem,
@@ -119,9 +119,10 @@
     mine = pl.multiple_of(sp * depth, depth)
     own_loads = [
         pltpu.make_async_copy(src, dst.at[pl.ds(mine, depth)], local_sem.at[4 + i])
-        for i, (src, dst) in enumerate(((wg_hbm, gate_w), (wu_hbm, up_w), (wd_hbm, down_w)))
+        for i, (src, dst) in enumerate(((wg_hbm, gate_w), (wu_hbm, up_w)))
     ]
-    for load in loads + own_loads:
+    down_load = pltpu.make_async_copy(wd_hbm, down_in, local_sem.at[6])
+    for load in loads + own_loads + [down_load]:
         load.start()
     pl.semaphore_wait(barrier, len(greeted))
 
@@ -157,8 +158,8 @@
     pieces = (
         (wg_hbm, gate_w, 0, depth),
         (wu_hbm, up_w, 0, depth),
-        (wd_hbm, down_w, 0, part_rows),
-        (wd_hbm, down_w, part_rows, part_rows),
+        (None, down_w, 0, part_rows),
+        (None, down_w, part_rows, part_rows),
     )
 
     def place(piece, chip_id, core_id):
@@ -168,6 +169,8 @@
 
     def own(piece):
         src, _, first, count = pieces[piece]
+        if src is None:
+            return place(piece, chip, core)
         return src.at[pl.ds(first, count)]
 
     def ring_out(way, piece, distance):
@@ -243,8 +246,10 @@
     launch(ring_out(1, 1, 1))
     launch(ring_out(0, 1, 1))
     launch(ring_out(1, 0, 1))
-    for piece in range(4):
+    for piece in (0, 1):
         launch(pair(0, piece, 0, core))
+    down_load.wait()
+    down_w[pl.ds(mine, depth), :] = down_in[...].T
 
     for load in loads[:3]:
         load.wait()
@@ -260,8 +265,9 @@
     )
     near = jnp.logical_and(offset >= 0, offset <= 2 * HALF)
     for block in range(rows // HALF):
-        doc_query = doc_col_ref[block * HALF : (block + 1) * HALF, :]
-        same = doc_query == doc_keys[:, block * HALF : block * HALF + reach]
+        doc_row = doc_all[:, (block + 1) * HALF : (block + 2) * HALF]
+        doc_query = jnp.broadcast_to(doc_row, (HALF, HALF)).T
+        same = jnp.concatenate([doc_query] * 3, 1) == doc_keys[:, block * HALF : block * HALF + reach]
         allowed = jnp.logical_and(near, same)
         for group in range(kv_local):
             lanes = slice(group * HEAD, (group + 1) * HEAD)
@@ -274,7 +280,7 @@
                     query_blk, key_blk, (((1,), (1,)), ((), ())), preferred_element_type=jnp.float32
                 ) * HEAD ** (-0.5)
                 scores = jnp.where(allowed, scores, NEGATIVE)
-                sink = sink_ref[h : h + 1, 0:1]
+                sink = jnp.full((1, 1), sink_ref[h], jnp.float32)
                 top = jnp.maximum(jnp.max(scores, -1, keepdims=True), sink)
                 weights = jnp.exp(scores - top)
                 total = jnp.sum(weights, -1, keepdims=True) + jnp.exp(sink - top)
@@ -284,6 +290,9 @@
                 att[block * HALF : (block + 1) * HALF, h * HEAD : (h + 1) * HEAD] = (
                     summed / total
                 ).astype(jnp.bfloat16)
+
+    for piece in (2, 3):
+        launch(pair(0, piece, 0, core))
 
     my_rows = pl.ds(pl.multiple_of(tp * token_rows, token_rows), token_rows)
     tokens[pl.ds(tp, 1)] = att[my_rows, :][None]
@@ -471,7 +480,7 @@
         return pl.pallas_call(
             functools.partial(kernel, sp_size, tp_size),
             out_shape=jax.ShapeDtypeStruct((token_rows, width), bf16),
-            in_specs=[vmem] * 6 + [anywhere] * 7,
+            in_specs=[vmem, pl.BlockSpec(memory_space=pltpu.SMEM)] + [vmem] * 3 + [anywhere] * 7,
             out_specs=vmem,
             scratch_shapes=[
                 pltpu.VMEM((span, keys.shape[1]), bf16),
@@ -486,6 +495,7 @@
                 pltpu.VMEM((token_rows, width), f32),
                 pltpu.VMEM((rows, width), bf16),
                 pltpu.VMEM((rows, units), bf16),
+                pltpu.VMEM(w_down.shape, bf16),
                 pltpu.VMEM((tp_size, token_rows, width), bf16),
                 pltpu.VMEM((others, token_rows, width), bf16),
                 dma((7,)),
@@ -507,8 +517,7 @@
             ),
         )(
             queries,
-            doc_ids[:, None],
-            jnp.broadcast_to(sink_logit[:, None], (sink_logit.shape[0], HEAD)),
+            sink_logit,
             residual_in,
             gain_one[None, :],
             gain_two[None, :],
@@ -518,7 +527,7 @@
             w_out,
             w_gate,
             w_up,
-            w_down.T,
+            w_down,
         )
 
     in_specs = (

time: 197 us -> 191 us (0.970)
  local copies, waits for them, and re-layouts: 7.39 us -> 2.3 us
    broadcast_in_dim x2 -> x0, local copies, waits for them, and re-layouts: 2.85 us -> none  [the longest x1 1.55 us: per_device(): doc_ids[:, None]]
    unnamed x2 -> x1, local copies, waits for them, and re-layouts: 4.54 us -> 2.3 us
where the time goes in v2:
time: 191 us
  Pallas kernels  189 us (99%)
  local copies, waits for them, and re-layouts  2.3 us (1%)
    pallas_call x1, Pallas kernels, per_device(): pl.pallas_call(functools.partial(kernel, sp_size, tp_size), out_shape=jax...  189 us

profile of v2, /device:TPU:0, one launch (start us, length us, event | category | flops | bytes accessed | tf_op | source)
XLA Modules:
  0.0 191.3 jit_solution(3197571697837327792)
XLA Ops:
  0.0 189.0 %shard_map.118 = bf16[256,2048]{1,0:T(8,128)(2,1)} custom-call(bf16[512,512]{1,0:T(8,128)(2,1)} %q_ref.1, f32[4]{0:T(128)} %sink_ref.1, bf16[256,2048]{1,0:T(8,128)(2,1)} %res_ref.1, f32[1,2048]{1,0:T(1,128)} %bitcast.3, f32[1,2048]{1,0:T(1,128)} %bitcast.4, bf16[512,256]{1,0:T(8,128)(2,1)} %k_hbm.1, bf16[512,256]{1,0:T(8,128)(2,1)} %v_hbm.1, ...), custom_call_target="tpu_custom_call" | custom-call | tf_op jit(solution)/shard_map/pallas_call | solution.py:480
  189.0 2.3 %copy.14 = bf16[256,2048]{1,0:T(8,128)(2,1)} copy(bf16[256,2048]{1,0:T(8,128)(2,1)} %shard_map.118) | data formatting | bytes 2097152
